TPU v7x, 512 devices: a whole 4x4x16 slice. The times are simulated.
512 devices in a mesh: ep: 16 (over y, x), tp: 32 (over z, core).
Axes of the slice: x: 4, y: 4, z: 16, core: 2. Of those that a mesh axis runs over, the one named last changes fastest.
Arguments:
- tokens: bfloat16 [3584, 4096], P('ep', 'tp'), may hold values from -6 to 6
- picks: int32 [16, 16, 56], P('ep'), may hold values from 0 to 223, as said below
- pick_weights: float32 [16, 16, 56], P('ep'), may hold values from 0.1 to 1
- gate_weight: bfloat16 [16, 1280, 4096], P('ep', 'tp'), may hold values from -0.09375 to 0.09375
- up_weight: bfloat16 [16, 1280, 4096], P('ep', 'tp'), may hold values from -0.09375 to 0.09375
- down_weight: bfloat16 [16, 1280, 4096], P('ep', None, 'tp'), may hold values from -0.15625 to 0.15625
- dense_gate: bfloat16 [5120, 4096], P('tp'), may hold values from -0.09375 to 0.09375
- dense_up: bfloat16 [5120, 4096], P('tp'), may hold values from -0.09375 to 0.09375
- dense_down: bfloat16 [5120, 4096], P('tp'), may hold values from -0.078125 to 0.078125
- branch_gate: float32 [4096], P('tp'), may hold values from -6 to 6
Outputs:
- mixed: bfloat16 [3584, 4096], P('ep', 'tp')
Inputs may be any that keep to these rules, and one draw needn't show every extreme that they name: For each block s and expert e, the 56 entries picks[s, e, :] are distinct rows of that block.
All inputs are finite; a program needn't handle non-finite values.
Results may differ from a plain program's by a relative error of at most 0.014.
Values may be sent and summed in bfloat16 or wider, within the bound.
No kernel may reach another device: no remote copies, remote signals or barrier semaphores. Data moves between devices by JAX's collectives and lax.ppermute only.
A program may use at most 64 MiB of HBM per device.

v0:
```python
import jax
import jax.numpy as jnp
from jax import lax
from jax.sharding import Mesh
from jax.sharding import PartitionSpec as P

TP = ("tp_0", "tp_1")


def copy_for_each(x, axis):
    copies = jnp.broadcast_to(x, (lax.axis_size(axis), *x.shape))
    return lax.all_to_all(copies, axis, split_axis=0, concat_axis=0, tiled=True)


def laid_out(tiles, dim):
    tiles = jnp.moveaxis(tiles, 0, dim)
    shape = tiles.shape
    return tiles.reshape(*shape[:dim], shape[dim] * shape[dim + 1], *shape[dim + 2 :])


def gather_directly(x, axis, dim):
    tiles = copy_for_each(x, axis)
    return laid_out(tiles, dim)


def stacked_from(x, axes, sequence):
    tiles = x[None]
    for k in sequence:
        tiles = lax.all_gather(tiles, axes[k], axis=0, tiled=True)
    carried = [lax.axis_size(axes[k]) for k in reversed(sequence)]
    tiles = tiles.reshape(*carried, *x.shape)
    turned = sorted(range(len(sequence)), key=lambda place: sequence[len(sequence) - 1 - place])
    return tiles.transpose(*turned, *range(len(sequence), tiles.ndim)).reshape(-1, *x.shape)


def whole_of(x, axes, sequence, dim):
    return laid_out(stacked_from(x, axes, sequence), dim)


def split_up(x, dim, peers):
    shape = x.shape
    tiles = x.reshape(*shape[:dim], peers, shape[dim] // peers, *shape[dim + 1 :])
    return jnp.moveaxis(tiles, dim, 0)


def summed_on_arrival(x, axis, dim):
    peers = lax.axis_size(axis)
    tiles = lax.all_to_all(split_up(x, dim, peers), axis, 0, 0, tiled=True)
    return jnp.sum(tiles.astype(jnp.float32), axis=0)


def per_device(
    tokens,
    picks,
    pick_weights,
    gate_weight,
    up_weight,
    down_weight,
    dense_gate,
    dense_up,
    dense_down,
    branch_gate,
):
    tok_rows = tokens.shape[0]
    experts = picks.shape[1]
    slots = picks.shape[2]
    chosen = picks.reshape(-1)
    full_rows = gather_directly(tokens, TP, 1)
    picked = jnp.take(tokens, chosen, axis=0).reshape(experts, slots, tokens.shape[1])
    landed = lax.all_to_all(picked, "ep", split_axis=0, concat_axis=0, tiled=True)
    arrived = whole_of(landed, TP, (0, 1), 2)
    expert_rows = arrived.reshape(-1, arrived.shape[2])
    contract_last = (((1,), (1,)), ((), ()))
    gate_value = lax.dot_general(
        gate_weight[0], expert_rows, contract_last, preferred_element_type=jnp.float32
    )
    up_value = lax.dot_general(
        up_weight[0], expert_rows, contract_last, preferred_element_type=jnp.float32
    )
    hidden = (jax.nn.silu(gate_value) * up_value).astype(jnp.bfloat16)
    columns = down_weight[0]
    expert_out = lax.dot_general(
        lax.all_gather(hidden, TP, axis=0, tiled=True),
        columns,
        (((0,), (0,)), ((), ())),
        preferred_element_type=jnp.float32,
    ).astype(jnp.bfloat16)
    sent_back = lax.all_to_all(
        expert_out.reshape(-1, slots, columns.shape[1]),
        "ep",
        split_axis=0,
        concat_axis=0,
        tiled=True,
    )
    row_ids = lax.broadcasted_iota(jnp.int32, (experts, tok_rows, slots), 1)
    matches = row_ids == picks[0][:, None, :]
    selector = matches.astype(jnp.bfloat16)
    token_weights = jnp.sum(jnp.where(matches, pick_weights[0][:, None, :], 0.0), axis=2)
    placed = jnp.einsum("ets,esd->etd", selector, sent_back, preferred_element_type=jnp.float32)
    mixture = jnp.sum(token_weights[:, :, None] * placed, axis=0)
    dense_gval = lax.dot_general(
        dense_gate, full_rows, contract_last, preferred_element_type=jnp.float32
    )
    dense_uval = lax.dot_general(
        dense_up, full_rows, contract_last, preferred_element_type=jnp.float32
    )
    dense_hidden = (jax.nn.silu(dense_gval) * dense_uval).astype(jnp.bfloat16)
    dense_part = summed_on_arrival(
        lax.dot_general(
            dense_down, dense_hidden, (((0,), (0,)), ((), ())), preferred_element_type=jnp.float32
        ).astype(jnp.bfloat16),
        TP,
        0,
    )
    mixed = mixture + jax.nn.sigmoid(branch_gate)[None, :] * jnp.transpose(dense_part)
    return mixed.astype(jnp.bfloat16)


def solution(mesh):
    split = Mesh(mesh.devices.reshape(mesh.shape["ep"], 16, 2), ("ep", "tp_0", "tp_1"))
    placed = (
        P("ep", TP),
        P("ep", None, None),
        P("ep", None, None),
        P("ep", TP, None),
        P("ep", TP, None),
        P("ep", None, TP),
        P(TP, None),
        P(TP, None),
        P(TP, None),
        P(TP),
    )
    return jax.shard_map(
        per_device, mesh=split, in_specs=placed, out_specs=P("ep", TP), check_vma=False
    )
```

profile of v0, /device:TPU:1, one launch (start us, length us, event | category | flops | bytes accessed | tf_op | source)
XLA Modules:
  0.0 334.2 jit_solution(6282708274561023143)
XLA Ops:
  6.5 0.9 reshape.63
  7.4 0.7 compare_and_fusion
  8.2 2.8 gather_fusion
  11.0 0.2 broadcast_select_fusion
  11.2 15.0 %all_to_all.20 = bf16[16,56,128]{2,1,0:T(8,128)(2,1)} all-to-all(bf16[16,56,128]{2,1,0:T(8,128)(2,1)S(1)} %broadcast_select_fusion), channel_id=1, replica_groups=mesh['ep'=16,'tp_0'=16,'tp_1'=2] {'ep'}, dimensions={0} | all-to-all | bytes 458752 | tf_op jit(solution)/shard_map/all_to_all | solution.py:70
  26.2 0.0 all-gather.9.cloned.1.call-update
  26.2 1.5 broadcast_in_dim.38
  27.7 17.2 %all-to-all-start.2 = ((bf16[32,224,128]{2,1,0:T(8,128)(2,1)}), bf16[32,224,128]{2,1,0:T(8,128)(2,1)S(1)}, u32[]{:S(2)}, u32[]{:S(2)}) async-start(bf16[32,224,128]{2,1,0:T(8,128)(2,1)} %broadcast_in_dim.38), calls=%async_computation.2 | async-start | bytes 3670016 | tf_op jit(solution)/shard_map/all_to_all | solution.py:12
  44.9 0.0 all-gather.5.cloned.1.call-start
  45.0 124.8 %all-gather.9.cloned.1.call-done = bf16[256,56,128]{2,1,0:T(8,128)(2,1)} async-done(((bf16[16,56,128]{2,1,0:T(8,128)(2,1)}), bf16[256,56,128]{2,1,0:T(8,128)(2,1)}) %all-gather.9.cloned.1.call-update) | async-done | bytes 3670032 | tf_op jit(solution)/shard_map/all_gather | solution.py:29
  169.8 0.0 all-gather.5.cloned.1.call-update
  169.9 2.1 fusion.8
  172.0 4.8 %fusion.12 = bf16[28,32,8,128]{3,2,1,0:T(8,128)(2,1)} fusion(bf16[160,4096]{1,0:T(8,128)(2,1)S(1)} %copy-done, bf16[160,4096]{1,0:T(8,128)(2,1)} %param.17, f32[160,224]{1,0:T(8,128)S(1)} %fusion.8, bf16[32,224,128]{2,1,0:T(8,128)(2,1)S(1)} %all-to-all-done.2), kind=kOutput, calls=%fused_computation.17 | convolution fusion | flops 588335104 | bytes 6434816 | tf_op jit(solution)/shard_map/dot_general | solution.py:109
  176.8 3.1 copy.52
  179.9 13.1 %all-to-all-start.3 = ((bf16[32,128,224]{1,2,0:T(8,128)(2,1)}), bf16[32,128,224]{1,2,0:T(8,128)(2,1)S(1)}, u32[]{:S(2)}, u32[]{:S(2)}) async-start(bf16[32,128,224]{1,2,0:T(8,128)(2,1)} %bitcast.78), calls=%async_computation.3 | async-start | bytes 3670016 | tf_op jit(solution)/shard_map/all_to_all | solution.py:48
  193.0 0.2 all-gather.7.cloned.1.call-start
  193.2 7.0 %all-gather.5.cloned.1.call-done = bf16[32,16,56,128]{3,2,1,0:T(8,128)(2,1)} async-done(((bf16[16,16,56,128]{3,2,1,0:T(8,128)(2,1)}), bf16[32,16,56,128]{3,2,1,0:T(8,128)(2,1)}) %all-gather.5.cloned.1.call-update) | async-done | bytes 7340048 | tf_op jit(solution)/shard_map/all_gather | solution.py:29
  200.2 5.1 %copy.14 = bf16[16,2,16,56,128]{4,3,2,1,0:T(8,128)(2,1)S(1)} copy(bf16[16,2,16,56,128]{4,3,2,0,1:T(8,128)(2,1)} %bitcast.80) | data formatting | bytes 14680064 | tf_op jit(solution)/shard_map/transpose | solution.py:33
  205.3 0.0 copy-start.5
  205.3 7.7 %copy.15 = bf16[16,56,32,128]{3,2,1,0:T(8,128)(2,1)} copy(bf16[16,56,32,128]{3,1,0,2:T(8,128)(2,1)S(1)} %bitcast.79) | data formatting | bytes 14680064 | tf_op jit(solution)/shard_map/transpose | solution.py:16
  213.0 5.5 %fusion.16 = f32[40,896]{1,0:T(8,128)S(1)} fusion(bf16[112,8,32,128]{3,2,1,0:T(8,128)(2,1)} %bitcast.81, bf16[1,40,4096]{2,1,0:T(8,128)(2,1)S(1)} %copy-done.5), kind=kOutput, calls=%fused_computation.20 | convolution fusion | flops 293601280 | bytes 7811072 | tf_op jit(solution)/shard_map/dot_general | solution.py:74
  218.6 0.0 copy-start.7
  218.6 3.0 fusion.28
  221.6 0.0 all-gather.7.cloned.1.call-update
  221.6 88.5 %all-gather.7.cloned.1.call-done = bf16[1280,896]{1,0:T(8,128)(2,1)} async-done(((bf16[40,896]{1,0:T(8,128)(2,1)}), bf16[1280,896]{1,0:T(8,128)(2,1)}) %all-gather.7.cloned.1.call-update) | async-done | bytes 2293776 | tf_op jit(solution)/shard_map/all_gather | solution.py:83
  310.1 3.2 convolution_convert_fusion.1
  313.3 4.6 %all-to-all-start.1 = ((bf16[16,56,128]{2,1,0:T(8,128)(2,1)}), bf16[16,56,128]{2,1,0:T(8,128)(2,1)S(1)}, u32[]{:S(2)}, u32[]{:S(2)}) async-start(bf16[16,56,128]{2,1,0:T(8,128)(2,1)} %bitcast.13), calls=%async_computation.1 | async-start | bytes 458752 | tf_op jit(solution)/shard_map/all_to_all | solution.py:88
  317.8 0.3 select_reduce_fusion
  318.2 0.3 convert_reduce_fusion
  318.4 7.2 %all-to-all-done.1 = bf16[16,56,128]{2,1,0:T(8,128)(2,1)S(1)} async-done(((bf16[16,56,128]{2,1,0:T(8,128)(2,1)}), bf16[16,56,128]{2,1,0:T(8,128)(2,1)S(1)}, u32[]{:S(2)}, u32[]{:S(2)}) %all-to-all-start.1) | async-done | bytes 229408 | tf_op jit(solution)/shard_map/all_to_all | solution.py:88
  325.7 1.3 multiply_reduce_fusion
  327.0 0.6 fusion.42
  (22 shorter events, 0.1 us)
Async XLA Ops:
  6.5 165.4 %copy-start = (bf16[160,4096]{1,0:T(8,128)(2,1)S(1)}, bf16[160,4096]{1,0:T(8,128)(2,1)}, u32[]{:S(2)}) copy-start(bf16[160,4096]{1,0:T(8,128)(2,1)} %param.18) | copy-start | bytes 3932164
  6.5 19.7 %copy-start.1 = (bf16[224,128]{1,0:T(8,128)(2,1)S(1)}, bf16[224,128]{1,0:T(8,128)(2,1)}, u32[]{:S(2)}) copy-start(bf16[224,128]{1,0:T(8,128)(2,1)} %param.10) | copy-start | bytes 172036
  6.5 163.3 %all-gather.9.cloned.1.call-start = ((), (), s32[]{:S(2)}) async-start(), calls=%async_computation.6 | async-start | bytes 3899392 | tf_op jit(solution)/shard_map/all_gather | solution.py:29
  27.7 142.1 %all-to-all-start.2 = ((bf16[32,224,128]{2,1,0:T(8,128)(2,1)}), bf16[32,224,128]{2,1,0:T(8,128)(2,1)S(1)}, u32[]{:S(2)}, u32[]{:S(2)}) async-start(bf16[32,224,128]{2,1,0:T(8,128)(2,1)} %broadcast_in_dim.38), calls=%async_computation.2 | async-start | bytes 3670016 | tf_op jit(solution)/shard_map/all_to_all | solution.py:12
  44.9 155.3 %all-gather.5.cloned.1.call-start = ((), (), s32[]{:S(2)}) async-start(), calls=%async_computation.4 | async-start | bytes 11010048 | tf_op jit(solution)/shard_map/all_gather | solution.py:29
  179.9 133.4 %all-to-all-start.3 = ((bf16[32,128,224]{1,2,0:T(8,128)(2,1)}), bf16[32,128,224]{1,2,0:T(8,128)(2,1)S(1)}, u32[]{:S(2)}, u32[]{:S(2)}) async-start(bf16[32,128,224]{1,2,0:T(8,128)(2,1)} %bitcast.78), calls=%async_computation.3 | async-start | bytes 3670016 | tf_op jit(solution)/shard_map/all_to_all | solution.py:48
  193.0 117.1 %all-gather.7.cloned.1.call-start = ((), (), s32[]{:S(2)}) async-start(), calls=%async_computation.5 | async-start | bytes 2365440 | tf_op jit(solution)/shard_map/all_gather | solution.py:83
  205.3 7.7 %copy-start.5 = (bf16[1,40,4096]{2,1,0:T(8,128)(2,1)S(1)}, bf16[1,40,4096]{2,1,0:T(8,128)(2,1)}, u32[]{:S(2)}) copy-start(bf16[1,40,4096]{2,1,0:T(8,128)(2,1)} %param.13) | copy-start | bytes 983044
  213.0 5.5 %copy-start.2 = (bf16[16,56,32,128]{3,2,1,0:T(8,128)(2,1)S(1)}, bf16[16,56,32,128]{3,2,1,0:T(8,128)(2,1)}, u32[]{:S(2)}) copy-start(bf16[16,56,32,128]{3,2,1,0:T(8,128)(2,1)} %copy.15) | copy-start | bytes 22020100
  213.0 5.5 %copy-start.6 = (bf16[1,40,4096]{2,1,0:T(8,128)(2,1)S(1)}, bf16[1,40,4096]{2,1,0:T(8,128)(2,1)}, u32[]{:S(2)}) copy-start(bf16[1,40,4096]{2,1,0:T(8,128)(2,1)} %param.14) | copy-start | bytes 983044
  218.6 3.0 copy-start.8
  218.6 91.5 %copy-start.7 = (bf16[1,1280,128]{2,1,0:T(8,128)(2,1)S(1)}, bf16[1,1280,128]{2,1,0:T(8,128)(2,1)}, u32[]{:S(2)}) copy-start(bf16[1,1280,128]{2,1,0:T(8,128)(2,1)} %param.15) | copy-start | bytes 983044
  221.6 96.2 %copy-start.3 = (s32[1,16,56]{2,1,0:T(8,128)S(1)}, s32[1,16,56]{2,1,0:T(8,128)}, u32[]{:S(2)}) copy-start(s32[1,16,56]{2,1,0:T(8,128)} %param.11) | copy-start | bytes 10756
  221.6 96.2 %copy-start.4 = (f32[1,16,56]{2,1,0:T(8,128)S(1)}, f32[1,16,56]{2,1,0:T(8,128)}, u32[]{:S(2)}) copy-start(f32[1,16,56]{2,1,0:T(8,128)} %param.12) | copy-start | bytes 10756
  313.3 12.4 %all-to-all-start.1 = ((bf16[16,56,128]{2,1,0:T(8,128)(2,1)}), bf16[16,56,128]{2,1,0:T(8,128)(2,1)S(1)}, u32[]{:S(2)}, u32[]{:S(2)}) async-start(bf16[16,56,128]{2,1,0:T(8,128)(2,1)} %bitcast.13), calls=%async_computation.1 | async-start | bytes 458752 | tf_op jit(solution)/shard_map/all_to_all | solution.py:88
Sparse Core Ops, SparseCore 0:
  26.3 143.4 all-gather.8
  171.9 28.2 all-gather.4
  221.7 88.3 all-gather.6
where the time goes:
time: 335 us; the launch traced here: 334 us
  waiting for transfers between devices  228 us (68%)
  starting transfers between devices  35.2 us (11%)
  local copies, waits for them, and re-layouts  21.1 us (6%)
  matrix products  19.9 us (6%)
  blocking collectives  15 us (4%)
  between operations  13.3 us (4%)
    all_gather x2, waiting for transfers between devices, stacked_from(): tiles = lax.all_gather(tiles, axes[k], axis=0, tiled=True)  132 us
    all_gather x1, waiting for transfers between devices, per_device(): lax.all_gather(hidden, TP, axis=0, tiled=True)  88.5 us
    all_to_all x1, starting transfers between devices, copy_for_each(): return lax.all_to_all(copies, axis, split_axis=0, concat_axis=0, tiled=True)  17.2 us
    all_to_all x1, blocking collectives, per_device(): lax.all_to_all(picked, 'ep', split_axis=0, concat_axis=0, tiled=True)  15 us
    all_to_all x1, starting transfers between devices, summed_on_arrival(): tiles = lax.all_to_all(split_up(x, dim, peers), axis, 0, 0, tiled=True)  13.1 us
    transpose x1, local copies, waits for them, and re-layouts, laid_out(): tiles = jnp.moveaxis(tiles, 0, dim)  7.66 us
    all_to_all x1, waiting for transfers between devices, per_device(): lax.all_to_all(expert_out.reshape(-1, slots, columns.shape[1]), 'ep', spl...  7.24 us
  transfers between devices with their start and end apart: 6, of which 4 were waited for; matrix products, arithmetic and copies ran while one was open for 11% of the time, Pallas kernels for 0%

commit v1 on v0

--- a/solution.py
+++ b/solution.py
@@ -26,7 +26,10 @@
 def stacked_from(x, axes, sequence):
     tiles = x[None]
     for k in sequence:
-        tiles = lax.all_gather(tiles, axes[k], axis=0, tiled=True)
+        size = lax.axis_size(axes[k])
+        tiles_2 = jnp.stack([tiles for _ in range(size)])
+        tiles_2 = lax.all_to_all(tiles_2, axes[k], split_axis=0, concat_axis=0)
+        tiles = jnp.concatenate(tiles_2, axis=0)
     carried = [lax.axis_size(axes[k]) for k in reversed(sequence)]
     tiles = tiles.reshape(*carried, *x.shape)
     turned = sorted(range(len(sequence)), key=lambda place: sequence[len(sequence) - 1 - place])

time: 335 us -> 464 us (1.39)
  blocking collectives: 15 us -> 134 us
  waiting for transfers between devices: 228 us -> 249 us
  starting transfers between devices: 35.2 us -> 19 us
    all_to_all x1, waiting for transfers between devices: 0.01 us -> 149 us  [stacked_from(): tiles_2 = lax.all_to_all(tiles_2, axes[k], split_axis=0, concat_axis=0)]
    all_gather x2 -> x0, waiting for transfers between devices: 132 us -> none  [stacked_from(): tiles = lax.all_gather(tiles, axes[k], axis=0, tiled=True)]
    all_to_all x0 -> x2, blocking collectives: none -> 119 us  [the longest x1 107 us: copy_for_each(): return lax.all_to_all(copies, axis, split_axis=0, concat_axis=0, tiled=True)]
    all_to_all x1, starting transfers between devices: 17.2 us -> 4.51 us  [stacked_from(): tiles_2 = lax.all_to_all(tiles_2, axes[k], split_axis=0, concat_axis=0)]
    all_to_all x0 -> x1, local copies, waits for them, and re-layouts: none -> 5.11 us  [stacked_from(): tiles_2 = lax.all_to_all(tiles_2, axes[k], split_axis=0, concat_axis=0)]
    transpose x1 -> x0, local copies, waits for them, and re-layouts: 5.11 us -> none  [stacked_from(): tiles.transpose(*turned, *range(len(sequence), tiles.ndim))]
  transfers between devices with their start and end apart: 6 -> 4, of which waited for: 4 -> 3; matrix products, arithmetic and copies ran while one was open for 11% -> 8% of each run, Pallas kernels for 0% -> 0%
where the time goes in v1:
time: 464 us; the launch traced here: 463 us
  waiting for transfers between devices  249 us (54%)
  blocking collectives  134 us (29%)
  local copies, waits for them, and re-layouts  22.5 us (5%)
  matrix products  19.9 us (4%)
  starting transfers between devices  19 us (4%)
  between operations  13.6 us (3%)
  other arithmetic  5.98 us (1%)
    all_to_all x1, waiting for transfers between devices, stacked_from(): tiles_2 = lax.all_to_all(tiles_2, axes[k], split_axis=0, concat_axis=0)  149 us
    all_to_all x1, blocking collectives, copy_for_each(): return lax.all_to_all(copies, axis, split_axis=0, concat_axis=0, tiled=True)  107 us
    all_gather x1, waiting for transfers between devices, per_device(): lax.all_gather(hidden, TP, axis=0, tiled=True)  92.1 us
    all_to_all x1, blocking collectives, per_device(): lax.all_to_all(picked, 'ep', split_axis=0, concat_axis=0, tiled=True)  14.7 us
    all_to_all x1, blocking collectives, stacked_from(): tiles_2 = lax.all_to_all(tiles_2, axes[k], split_axis=0, concat_axis=0)  12 us
    all_to_all x1, starting transfers between devices, summed_on_arrival(): tiles = lax.all_to_all(split_up(x, dim, peers), axis, 0, 0, tiled=True)  10.7 us
  transfers between devices with their start and end apart: 4, of which 3 were waited for; matrix products, arithmetic and copies ran while one was open for 8% of the time, Pallas kernels for 0%

profile of v1, /device:TPU:1, one launch (start us, length us, event | category | flops | bytes accessed | tf_op | source)
XLA Modules:
  0.0 463.2 jit_solution(11851258625476783091)
XLA Ops:
  6.5 0.9 reshape.62
  7.4 0.7 compare_and_fusion
  8.2 2.8 gather_fusion
  11.0 0.2 broadcast_select_fusion
  11.2 14.7 %all_to_all.30 = bf16[16,56,128]{2,1,0:T(8,128)(2,1)S(1)} all-to-all(bf16[16,56,128]{2,1,0:T(8,128)(2,1)S(1)} %broadcast_select_fusion), channel_id=1, replica_groups=mesh['ep'=16,'tp_0'=16,'tp_1'=2] {'ep'}, dimensions={0} | all-to-all | bytes 458752 | tf_op jit(solution)/shard_map/all_to_all | solution.py:73
  25.9 0.2 broadcast_in_dim.34
  26.2 106.7 %all_to_all.31 = bf16[32,224,128]{2,1,0:T(8,128)(2,1)S(1)} all-to-all(bf16[32,224,128]{2,1,0:T(8,128)(2,1)S(1)} %broadcast_in_dim.34), channel_id=1, replica_groups=mesh['ep'=16,'tp_0'=16,'tp_1'=2] {'tp_0','tp_1'}, dimensions={0} | all-to-all | bytes 3670016 | tf_op jit(solution)/shard_map/all_to_all | solution.py:12
  132.9 2.6 stack.6
  135.5 4.5 all-to-all-start.1
  140.0 2.1 fusion.8
  142.1 4.8 %fusion.12 = bf16[28,32,8,128]{3,2,1,0:T(8,128)(2,1)} fusion(bf16[160,4096]{1,0:T(8,128)(2,1)S(1)} %copy-done, bf16[160,4096]{1,0:T(8,128)(2,1)} %param.17, f32[160,224]{1,0:T(8,128)S(1)} %fusion.8, bf16[32,224,128]{2,1,0:T(8,128)(2,1)S(1)} %all_to_all.31), kind=kOutput, calls=%fused_computation.18 | convolution fusion | flops 588335104 | bytes 6434816 | tf_op jit(solution)/shard_map/dot_general | solution.py:112
  146.9 3.1 copy.50
  150.0 149.3 %all-to-all-done.1 = bf16[16,1,16,56,128]{4,3,2,1,0:T(8,128)(2,1)} async-done(((bf16[16,1,16,56,128]{4,3,2,1,0:T(8,128)(2,1)}), bf16[16,1,16,56,128]{4,3,2,1,0:T(8,128)(2,1)}, u32[]{:S(2)}, u32[]{:S(2)}) %all-to-all-start.1) | async-done | bytes 3670048 | tf_op jit(solution)/shard_map/all_to_all | solution.py:31
  299.3 3.8 pad_maximum_fusion
  303.1 12.0 %all_to_all.32 = bf16[2,16,16,56,128]{4,3,2,1,0:T(8,128)(2,1)} all-to-all(bf16[2,16,16,56,128]{4,3,2,1,0:T(8,128)(2,1)S(1)} %pad_maximum_fusion), channel_id=1, replica_groups=mesh['ep'=16,'tp_0'=16,'tp_1'=2] {'tp_1'}, dimensions={0} | all-to-all | bytes 14680064 | tf_op jit(solution)/shard_map/all_to_all | solution.py:31
  315.2 10.7 %all-to-all-start.5 = ((bf16[32,128,224]{1,2,0:T(8,128)(2,1)}), bf16[32,128,224]{1,2,0:T(8,128)(2,1)S(1)}, u32[]{:S(2)}, u32[]{:S(2)}) async-start(bf16[32,128,224]{1,2,0:T(8,128)(2,1)} %bitcast.77), calls=%async_computation.5 | async-start | bytes 3670016 | tf_op jit(solution)/shard_map/all_to_all | solution.py:51
  325.9 0.2 all-gather.2.cloned.1.call-start
  326.1 5.1 %copy.12 = bf16[2,16,16,56,128]{4,3,2,0,1:T(8,128)(2,1)S(1)} copy(bf16[2,16,16,56,128]{4,3,2,1,0:T(8,128)(2,1)} %all_to_all.32) | data formatting | bytes 14680064 | tf_op jit(solution)/shard_map/all_to_all | solution.py:31
  331.2 0.0 copy-start.5
  331.2 7.7 %copy.13 = bf16[16,56,32,128]{3,2,1,0:T(8,128)(2,1)} copy(bf16[16,56,32,128]{3,1,0,2:T(8,128)(2,1)S(1)} %bitcast.78) | data formatting | bytes 14680064 | tf_op jit(solution)/shard_map/transpose | solution.py:16
  338.9 5.5 %fusion.16 = f32[40,896]{1,0:T(8,128)S(1)} fusion(bf16[112,8,32,128]{3,2,1,0:T(8,128)(2,1)} %bitcast.79, bf16[1,40,4096]{2,1,0:T(8,128)(2,1)S(1)} %copy-done.5), kind=kOutput, calls=%fused_computation.21 | convolution fusion | flops 293601280 | bytes 7811072 | tf_op jit(solution)/shard_map/dot_general | solution.py:77
  344.5 0.0 copy-start.7
  344.5 3.0 fusion.28
  347.4 0.0 all-gather.2.cloned.1.call-update
  347.5 92.1 %all-gather.2.cloned.1.call-done = bf16[1280,896]{1,0:T(8,128)(2,1)} async-done(((bf16[40,896]{1,0:T(8,128)(2,1)}), bf16[1280,896]{1,0:T(8,128)(2,1)}) %all-gather.2.cloned.1.call-update) | async-done | bytes 2293776 | tf_op jit(solution)/shard_map/all_gather | solution.py:86
  439.6 3.2 convolution_convert_fusion.1
  442.8 3.5 all-to-all-start.3
  446.3 0.3 select_reduce_fusion
  446.7 0.3 convert_reduce_fusion
  446.9 7.5 %all-to-all-done.3 = bf16[16,56,128]{2,1,0:T(8,128)(2,1)S(1)} async-done(((bf16[16,56,128]{2,1,0:T(8,128)(2,1)}), bf16[16,56,128]{2,1,0:T(8,128)(2,1)S(1)}, u32[]{:S(2)}, u32[]{:S(2)}) %all-to-all-start.3) | async-done | bytes 229408 | tf_op jit(solution)/shard_map/all_to_all | solution.py:91
  454.4 1.3 multiply_reduce_fusion
  455.8 0.6 fusion.42
  (20 shorter events, 0.1 us)
Async XLA Ops:
  6.5 135.5 %copy-start = (bf16[160,4096]{1,0:T(8,128)(2,1)S(1)}, bf16[160,4096]{1,0:T(8,128)(2,1)}, u32[]{:S(2)}) copy-start(bf16[160,4096]{1,0:T(8,128)(2,1)} %param.18) | copy-start | bytes 3932164
  6.5 19.4 %copy-start.1 = (bf16[224,128]{1,0:T(8,128)(2,1)S(1)}, bf16[224,128]{1,0:T(8,128)(2,1)}, u32[]{:S(2)}) copy-start(bf16[224,128]{1,0:T(8,128)(2,1)} %param.10) | copy-start | bytes 172036
  135.5 163.8 %all-to-all-start.1 = ((bf16[16,1,16,56,128]{4,3,2,1,0:T(8,128)(2,1)}), bf16[16,1,16,56,128]{4,3,2,1,0:T(8,128)(2,1)}, u32[]{:S(2)}, u32[]{:S(2)}) async-start(bf16[16,1,16,56,128]{4,3,2,1,0:T(8,128)(2,1)} %stack.6), calls=%async_computation.1 | async-start | bytes 7340032 | tf_op jit(solution)/shard_map/all_to_all | solution.py:31
  315.2 127.6 %all-to-all-start.5 = ((bf16[32,128,224]{1,2,0:T(8,128)(2,1)}), bf16[32,128,224]{1,2,0:T(8,128)(2,1)S(1)}, u32[]{:S(2)}, u32[]{:S(2)}) async-start(bf16[32,128,224]{1,2,0:T(8,128)(2,1)} %bitcast.77), calls=%async_computation.5 | async-start | bytes 3670016 | tf_op jit(solution)/shard_map/all_to_all | solution.py:51
  325.9 113.7 %all-gather.2.cloned.1.call-start = ((), (), s32[]{:S(2)}) async-start(), calls=%async_computation.6 | async-start | bytes 2365440 | tf_op jit(solution)/shard_map/all_gather | solution.py:86
  331.2 7.7 %copy-start.5 = (bf16[1,40,4096]{2,1,0:T(8,128)(2,1)S(1)}, bf16[1,40,4096]{2,1,0:T(8,128)(2,1)}, u32[]{:S(2)}) copy-start(bf16[1,40,4096]{2,1,0:T(8,128)(2,1)} %param.13) | copy-start | bytes 983044
  338.9 5.5 %copy-start.2 = (bf16[16,56,32,128]{3,2,1,0:T(8,128)(2,1)S(1)}, bf16[16,56,32,128]{3,2,1,0:T(8,128)(2,1)}, u32[]{:S(2)}) copy-start(bf16[16,56,32,128]{3,2,1,0:T(8,128)(2,1)} %copy.13) | copy-start | bytes 22020100
  338.9 5.5 %copy-start.6 = (bf16[1,40,4096]{2,1,0:T(8,128)(2,1)S(1)}, bf16[1,40,4096]{2,1,0:T(8,128)(2,1)}, u32[]{:S(2)}) copy-start(bf16[1,40,4096]{2,1,0:T(8,128)(2,1)} %param.14) | copy-start | bytes 983044
  344.5 3.0 copy-start.8
  344.5 95.1 %copy-start.7 = (bf16[1,1280,128]{2,1,0:T(8,128)(2,1)S(1)}, bf16[1,1280,128]{2,1,0:T(8,128)(2,1)}, u32[]{:S(2)}) copy-start(bf16[1,1280,128]{2,1,0:T(8,128)(2,1)} %param.15) | copy-start | bytes 983044
  347.5 98.8 %copy-start.3 = (s32[1,16,56]{2,1,0:T(8,128)S(1)}, s32[1,16,56]{2,1,0:T(8,128)}, u32[]{:S(2)}) copy-start(s32[1,16,56]{2,1,0:T(8,128)} %param.11) | copy-start | bytes 10756
  347.5 98.8 %copy-start.4 = (f32[1,16,56]{2,1,0:T(8,128)S(1)}, f32[1,16,56]{2,1,0:T(8,128)}, u32[]{:S(2)}) copy-start(f32[1,16,56]{2,1,0:T(8,128)} %param.12) | copy-start | bytes 10756
  442.8 11.6 %all-to-all-start.3 = ((bf16[16,56,128]{2,1,0:T(8,128)(2,1)}), bf16[16,56,128]{2,1,0:T(8,128)(2,1)S(1)}, u32[]{:S(2)}, u32[]{:S(2)}) async-start(bf16[16,56,128]{2,1,0:T(8,128)(2,1)} %bitcast.12), calls=%async_computation.3 | async-start | bytes 458752 | tf_op jit(solution)/shard_map/all_to_all | solution.py:91
Sparse Core Ops, SparseCore 0:
  347.6 91.9 all-gather.1
